TPU v7x, 512 devices: a whole 4x4x16 slice. The times are simulated.
512 devices in a mesh: sp: 128 (over z, x, core), tp: 4 (over y).
Axes of the slice: x: 4, y: 4, z: 16, core: 2. Of those that a mesh axis runs over, the one named last changes fastest.
Arguments:
- tokens: bfloat16 [49152, 2048], P('sp'), may hold values from -6 to 6
- doc_ids: int32 [49152], P('sp'), may hold values from 0 to 31, never falling along the last dimension, each value on 1 to 3072 neighbouring positions
- pre_gain: float32 [2, 2048], replicated, may hold values from 0.1 to 1.9
- value_proj: bfloat16 [2, 2048, 1024], P(None, 'sp', 'tp'), may hold values from -0.5 to 0.5
- gate_proj: bfloat16 [2, 2048, 1024], P(None, 'sp', 'tp'), may hold values from -0.5 to 0.5
- out_proj: bfloat16 [2, 1024, 2048], P(None, 'tp', 'sp'), may hold values from -0.1875 to 0.1875
- conv_taps: float32 [2, 31, 1024], P(None, None, 'tp'), may hold values from -2.2 to 2.2
- norm_gain: float32 [2, 1024], P(None, 'tp'), may hold values from 0.1 to 1.9
- norm_shift: float32 [2, 1024], P(None, 'tp'), may hold values from -3 to 3
Outputs:
- hidden: bfloat16 [49152, 2048], P('sp')
Inputs may be any that keep to these rules, and one draw needn't show every extreme that they name: `doc_ids`: document numbers never fall along the sequence; each document has 1 to 3072 positions.
All inputs are finite; a program needn't handle non-finite values.
Results may differ from a plain program's by a relative error of at most 0.017.
Values may be sent and summed in bfloat16 or wider, within the bound.
A program may use at most 64 MiB of HBM per device.

v0:
```python
import jax
import jax.numpy as jnp
from jax import lax
from jax.sharding import PartitionSpec as P

epsilon = 1e-06


def rows_first(arrays, axis, dims):
    turned = [jnp.moveaxis(a, dim, 0) for a, dim in zip(arrays, dims)]
    both = jnp.concatenate([t.reshape(len(t), -1) for t in turned], axis=1)
    out, at, outs = (lax.all_gather(both, axis, axis=0, tiled=True), 0, [])
    for t, dim in zip(turned, dims):
        slab = out[:, at : at + t[0].size].reshape(-1, *t.shape[1:])
        outs.append(jnp.moveaxis(slab, 0, dim))
        at += t[0].size
    return tuple(outs)


def passed_along(value, axis, steps):
    count = lax.axis_size(axis)
    first, last = (max(0, -steps), min(count, count - steps))
    return lax.ppermute(value, axis, [(source, source + steps) for source in range(first, last)])


def sent_to_all(value, axis):
    copies = jnp.broadcast_to(value, (lax.axis_size(axis), *value.shape))
    return lax.all_to_all(copies, axis, split_axis=0, concat_axis=0, tiled=True)


def taken_together(value, axis):
    everything = sent_to_all(value, axis)
    return jnp.sum(everything, axis=0)


def together(arrays, axis):
    ravelled, at, outs = (jnp.concatenate([a.reshape(-1) for a in arrays]), 0, [])
    total = taken_together(ravelled, axis)
    for a in arrays:
        outs.append(total[at : at + a.size].reshape(a.shape))
        at += a.size
    return tuple(outs)


def cut_along(value, dim, length):
    before, after = (value.shape[:dim], value.shape[dim + 1 :])
    return jnp.moveaxis(value.reshape(*before, length, -1, *after), dim, 0)


def summed_on_arrival(value, axis, dim):
    pieces = cut_along(value, dim, lax.axis_size(axis))
    arrived = lax.all_to_all(pieces, axis, split_axis=0, concat_axis=0, tiled=True)
    return arrived.astype(jnp.float32).sum(axis=0)


def in_order(pieces, dim):
    lengths = list(pieces.shape[1:])
    lengths[dim] *= pieces.shape[0]
    return jnp.moveaxis(pieces, 0, dim).reshape(lengths)


def collect(value, axis, dim):
    return in_order(sent_to_all(value, axis), dim)


def on_device(
    tokens, doc_ids, pre_gain, value_proj, gate_proj, out_proj, conv_taps, norm_gain, norm_shift
):
    layer_count = value_proj.shape[0]
    tap_count = conv_taps.shape[1]
    reach_rows = tap_count - 1
    row_count = tokens.shape[0]
    block_width = conv_taps.shape[2]
    channels = block_width * lax.axis_size("tp")
    hidden = tokens
    full_value, full_gate, full_out = rows_first((value_proj, gate_proj, out_proj), "sp", (1, 1, 2))
    for layer_index in range(layer_count):
        wide_state = hidden.astype(jnp.float32)
        scale = lax.rsqrt(jnp.mean(wide_state * wide_state, axis=-1, keepdims=True) + epsilon)
        normed = (wide_state * scale * pre_gain[layer_index]).astype(jnp.bfloat16)
        value_acc = jnp.dot(normed, full_value[layer_index], preferred_element_type=jnp.float32)
        gate_acc = jnp.dot(normed, full_gate[layer_index], preferred_element_type=jnp.float32)
        value_half = value_acc.astype(jnp.bfloat16)
        gate_half = gate_acc.astype(jnp.bfloat16)
        gated_rows = (
            value_half.astype(jnp.float32) * jax.nn.sigmoid(gate_half.astype(jnp.float32))
        ).astype(jnp.bfloat16)
        prev_rows, prev_docs = passed_along(
            (gated_rows[row_count - reach_rows :], doc_ids[row_count - reach_rows :]), "sp", 1
        )
        padded = jnp.concatenate([prev_rows, gated_rows]).astype(jnp.float32)
        padded_docs = jnp.concatenate([prev_docs, doc_ids])
        conv_out = jnp.zeros((row_count, block_width), jnp.float32)
        for offset in range(tap_count):
            first_row = reach_rows - offset
            same_doc = (padded_docs[first_row : first_row + row_count] == doc_ids)[:, None]
            term = (
                conv_taps[layer_index, offset][None, :] * padded[first_row : first_row + row_count]
            )
            conv_out = conv_out + jnp.where(same_doc, term, jnp.float32(0.0))
        row_sums, square_sums = together(
            (jnp.sum(conv_out, axis=1), jnp.sum(conv_out * conv_out, axis=1)), "tp"
        )
        row_mean = (row_sums / channels)[:, None]
        row_var = (square_sums / channels)[:, None] - row_mean * row_mean
        normalized = (
            norm_gain[layer_index] * (conv_out - row_mean) * lax.rsqrt(row_var + epsilon)
            + norm_shift[layer_index]
        )
        activated = jax.nn.silu(normalized).astype(jnp.bfloat16)
        partial_value = jnp.dot(
            activated, full_out[layer_index], preferred_element_type=jnp.float32
        )
        summed = summed_on_arrival(partial_value.astype(jnp.bfloat16), "tp", 1)
        branch = summed.astype(jnp.bfloat16)
        piece_width = summed.shape[1]
        own_cols = lax.dynamic_slice_in_dim(
            hidden, lax.axis_index("tp") * piece_width, piece_width, 1
        )
        updated = (own_cols.astype(jnp.float32) + branch.astype(jnp.float32)).astype(jnp.bfloat16)
        hidden = collect(updated, "tp", 1)
    return hidden


def solution(mesh):
    return jax.shard_map(
        on_device,
        mesh=mesh,
        in_specs=(
            P("sp", None),
            P("sp"),
            P(),
            P(None, "sp", "tp"),
            P(None, "sp", "tp"),
            P(None, "tp", "sp"),
            P(None, None, "tp"),
            P(None, "tp"),
            P(None, "tp"),
        ),
        out_specs=P("sp", None),
        check_vma=False,
    )
```

profile of v0, /device:TPU:36, one launch (start us, length us, event | category | flops | bytes accessed | tf_op | source)
XLA Modules:
  0.0 315.1 jit_solution(1334254646113636902)
XLA Ops:
  10.1 1.9 collective-permute-start.1
  12.0 1.8 fusion
  19.5 137.9 %all-gather.2.cloned.1.call-done = bf16[2048,1536]{1,0:T(8,128)(2,1)} async-done(((bf16[16,1536]{1,0:T(8,128)(2,1)}), bf16[2048,1536]{1,0:T(8,128)(2,1)}) %all-gather.2.cloned.1.call-update) | async-done | bytes 6291472 | tf_op jit(solution)/shard_map/all_gather | solution.py:12
  157.4 3.4 %fusion.160 = (bf16[2048,512]{1,0:T(8,128)(2,1)S(1)}, bf16[2048,512]{1,0:T(8,128)(2,1)S(1)}, bf16[2048,512]{1,0:T(8,128)(2,1)S(1)}) fusion(bf16[2048,1536]{1,0:T(8,128)(2,1)} %all-gather.2.cloned.1.call-done), kind=kLoop, calls=%fused_computation.288 | loop fusion | bytes 12582912 | tf_op jit(solution)/shard_map/slice | solution.py:14
  164.9 2.1 collective-permute-start
  167.1 2.8 collective-permute-done
  170.0 3.3 %fusion.157 = (f32[384]{0:T(512)S(1)}, f32[384]{0:T(512)S(1)}, f32[384,256]{1,0:T(8,128)S(1)}) fusion(f32[414,256]{1,0:T(8,128)S(1)} %maximum_convert_fusion, f32[256]{0:T(256)S(1)} %bitcast.193, pred[384]{0:T(512)(128)(4,1)S(1)} %get-tuple-element.110, f32[256]{0:T(256)S(1)} %bitcast.194, pred[384]{0:T(512)(128)(4,1)S(1)} %get-tuple-element.111, ...), kind=kLoop, calls=%fused_computation.287 | loop fusion | flops 9239808 | bytes 12629248 | tf_op jit(solution)/shard_map/reduce_sum | solution.py:102
  174.0 4.2 %all-to-all-start = ((f32[4,1,768]{2,1,0:T(1,128)}), f32[4,1,768]{2,1,0:T(1,128)S(1)}, u32[]{:S(2)}, u32[]{:S(2)}) async-start(f32[4,1,768]{2,1,0:T(1,128)} %broadcast_in_dim.423), calls=%async_computation | async-start | bytes 24576 | tf_op jit(solution)/shard_map/all_to_all | solution.py:28
  178.2 2.5 copy.74
  180.6 2.9 all-to-all-done
  183.5 1.9 convolution_convert_fusion.1
  186.7 3.6 %all-to-all-start.1 = ((bf16[4,384,512]{2,1,0:T(8,128)(2,1)}), bf16[4,384,512]{2,1,0:T(8,128)(2,1)S(1)}, u32[]{:S(2)}, u32[]{:S(2)}) async-start(bf16[4,384,512]{2,1,0:T(8,128)(2,1)} %bitcast.135), calls=%async_computation.1 | async-start | bytes 3145728 | tf_op jit(solution)/shard_map/all_to_all | solution.py:52
  190.3 18.3 %all-to-all-done.1 = bf16[4,384,512]{2,1,0:T(8,128)(2,1)S(1)} async-done(((bf16[4,384,512]{2,1,0:T(8,128)(2,1)}), bf16[4,384,512]{2,1,0:T(8,128)(2,1)S(1)}, u32[]{:S(2)}, u32[]{:S(2)}) %all-to-all-start.1) | async-done | bytes 1572896 | tf_op jit(solution)/shard_map/all_to_all | solution.py:52
  211.4 3.6 %all-to-all-start.2 = ((bf16[4,384,512]{2,1,0:T(8,128)(2,1)}), bf16[4,384,512]{2,1,0:T(8,128)(2,1)S(1)}, u32[]{:S(2)}, u32[]{:S(2)}) async-start(bf16[4,384,512]{2,1,0:T(8,128)(2,1)} %broadcast_in_dim.424), calls=%async_computation.2 | async-start | bytes 3145728 | tf_op jit(solution)/shard_map/all_to_all | solution.py:28
  215.0 17.5 %all-to-all-done.2 = bf16[4,384,512]{2,1,0:T(8,128)(2,1)S(1)} async-done(((bf16[4,384,512]{2,1,0:T(8,128)(2,1)}), bf16[4,384,512]{2,1,0:T(8,128)(2,1)S(1)}, u32[]{:S(2)}, u32[]{:S(2)}) %all-to-all-start.2) | async-done | bytes 1572896 | tf_op jit(solution)/shard_map/all_to_all | solution.py:28
  236.6 1.9 collective-permute-start.2
  239.4 2.2 collective-permute-done.2
  241.7 3.3 %fusion.156 = (f32[384]{0:T(512)S(1)}, f32[384]{0:T(512)S(1)}, f32[384,256]{1,0:T(8,128)S(1)}) fusion(f32[414,256]{1,0:T(8,128)S(1)} %maximum_convert_fusion.1, f32[256]{0:T(256)S(1)} %bitcast.159, pred[384]{0:T(512)(128)(4,1)S(1)} %get-tuple-element.110, f32[256]{0:T(256)S(1)} %bitcast.160, pred[384]{0:T(512)(128)(4,1)S(1)} %get-tuple-element.111, ...), kind=kLoop, calls=%fused_computation.286 | loop fusion | flops 9239808 | bytes 12629248 | tf_op jit(solution)/shard_map/reduce_sum | solution.py:102
  245.1 7.7 %all_to_all.32 = f32[4,1,768]{2,1,0:T(1,128)S(1)} all-to-all(f32[4,1,768]{2,1,0:T(1,128)S(1)} %broadcast_in_dim.425), channel_id=1, replica_groups=mesh['sp'=128,'tp'=4] {'tp'}, dimensions={0} | all-to-all | bytes 24576 | tf_op jit(solution)/shard_map/all_to_all | solution.py:28
  252.8 1.9 convolution_convert_fusion
  255.9 3.6 %all-to-all-start.4 = ((bf16[4,384,512]{2,1,0:T(8,128)(2,1)}), bf16[4,384,512]{2,1,0:T(8,128)(2,1)S(1)}, u32[]{:S(2)}, u32[]{:S(2)}) async-start(bf16[4,384,512]{2,1,0:T(8,128)(2,1)} %bitcast.139), calls=%async_computation.4 | async-start | bytes 3145728 | tf_op jit(solution)/shard_map/all_to_all | solution.py:52
  259.8 21.7 %all-to-all-done.4 = bf16[4,384,512]{2,1,0:T(8,128)(2,1)S(1)} async-done(((bf16[4,384,512]{2,1,0:T(8,128)(2,1)}), bf16[4,384,512]{2,1,0:T(8,128)(2,1)S(1)}, u32[]{:S(2)}, u32[]{:S(2)}) %all-to-all-start.4) | async-done | bytes 1572896 | tf_op jit(solution)/shard_map/all_to_all | solution.py:52
  282.2 23.6 %all_to_all.33 = bf16[4,384,512]{2,1,0:T(8,128)(2,1)S(1)} all-to-all(bf16[4,384,512]{2,1,0:T(8,128)(2,1)S(1)} %broadcast_in_dim.426), channel_id=1, replica_groups=mesh['sp'=128,'tp'=4] {'tp'}, dimensions={0} | all-to-all | bytes 3145728 | tf_op jit(solution)/shard_map/all_to_all | solution.py:28
  306.6 1.6 copy.73
  (67 shorter events, 26.1 us)
Async XLA Ops:
  6.5 150.9 %all-gather.2.cloned.1.call-start = ((), (), s32[]{:S(2)}) async-start(), calls=%async_computation.6 | async-start | bytes 6340608 | tf_op jit(solution)/shard_map/all_gather | solution.py:12
  10.1 7.8 %collective-permute-start.1 = (s32[30]{0:T(128)S(1)}, s32[30]{0:T(128)S(1)}, u32[]{:S(2)}, u32[]{:S(2)}) collective-permute-start(s32[30]{0:T(128)S(1)} %slice.568), channel_id=1, source_target_pairs={{0,4},{4,8},{8,12},{12,16},{16,20},{20,24},{24,28},{28,32},{32,36}... | collective-permute-start | bytes 368 | tf_op jit(solution)/shard_map/ppermute | solution.py:23
  161.0 1.3 copy-start
  161.0 2.6 copy-start.2
  161.1 3.1 copy-start.3
  164.2 2.8 copy-start.5
  164.9 5.1 %collective-permute-start = (bf16[30,256]{1,0:T(8,128)(2,1)S(1)}, bf16[30,256]{1,0:T(8,128)(2,1)S(1)}, u32[]{:S(2)}, u32[]{:S(2)}) collective-permute-start(bf16[30,256]{1,0:T(8,128)(2,1)S(1)} %slice.739), channel_id=1, source_target_pairs={{0,4},{4,8},{8,12},{12,16},{16,20},{20,24},{24,28},{28,32},{32,36}... | collective-permute-start | bytes 46088 | tf_op jit(solution)/shard_map/ppermute | solution.py:23
  170.0 8.2 %copy-start.6 = (f32[2,256]{1,0:T(2,128)S(1)}, f32[2,256]{1,0:T(2,128)}, u32[]{:S(2)}) copy-start(f32[2,256]{1,0:T(2,128)} %param.17) | copy-start | bytes 6148
  174.0 9.6 %all-to-all-start = ((f32[4,1,768]{2,1,0:T(1,128)}), f32[4,1,768]{2,1,0:T(1,128)S(1)}, u32[]{:S(2)}, u32[]{:S(2)}) async-start(f32[4,1,768]{2,1,0:T(1,128)} %broadcast_in_dim.423), calls=%async_computation | async-start | bytes 24576 | tf_op jit(solution)/shard_map/all_to_all | solution.py:28
  186.7 21.9 %all-to-all-start.1 = ((bf16[4,384,512]{2,1,0:T(8,128)(2,1)}), bf16[4,384,512]{2,1,0:T(8,128)(2,1)S(1)}, u32[]{:S(2)}, u32[]{:S(2)}) async-start(bf16[4,384,512]{2,1,0:T(8,128)(2,1)} %bitcast.135), calls=%async_computation.1 | async-start | bytes 3145728 | tf_op jit(solution)/shard_map/all_to_all | solution.py:52
  211.4 21.0 %all-to-all-start.2 = ((bf16[4,384,512]{2,1,0:T(8,128)(2,1)}), bf16[4,384,512]{2,1,0:T(8,128)(2,1)S(1)}, u32[]{:S(2)}, u32[]{:S(2)}) async-start(bf16[4,384,512]{2,1,0:T(8,128)(2,1)} %broadcast_in_dim.424), calls=%async_computation.2 | async-start | bytes 3145728 | tf_op jit(solution)/shard_map/all_to_all | solution.py:28
  233.3 1.6 copy-start.1
  234.2 1.7 copy-start.4
  236.6 5.1 %collective-permute-start.2 = (bf16[30,256]{1,0:T(8,128)(2,1)S(1)}, bf16[30,256]{1,0:T(8,128)(2,1)S(1)}, u32[]{:S(2)}, u32[]{:S(2)}) collective-permute-start(bf16[30,256]{1,0:T(8,128)(2,1)S(1)} %slice.775), channel_id=1, source_target_pairs={{0,4},{4,8},{8,12},{12,16},{16,20},{20,24},{24,28},{28,32},{32,36}... | collective-permute-start | bytes 46088 | tf_op jit(solution)/shard_map/ppermute | solution.py:23
  255.9 25.5 %all-to-all-start.4 = ((bf16[4,384,512]{2,1,0:T(8,128)(2,1)}), bf16[4,384,512]{2,1,0:T(8,128)(2,1)S(1)}, u32[]{:S(2)}, u32[]{:S(2)}) async-start(bf16[4,384,512]{2,1,0:T(8,128)(2,1)} %bitcast.139), calls=%async_computation.4 | async-start | bytes 3145728 | tf_op jit(solution)/shard_map/all_to_all | solution.py:52
Sparse Core Ops, SparseCore 0:
  10.5 146.8 all-gather.1
where the time goes:
time: 316 us; the launch traced here: 315 us
  waiting for transfers between devices  203 us (64%)
  blocking collectives  31.3 us (10%)
  local copies, waits for them, and re-layouts  25.7 us (8%)
  starting transfers between devices  20.9 us (7%)
  between operations  13.8 us (4%)
  other arithmetic  13.7 us (4%)
  matrix products  6.31 us (2%)
    all_gather x1, waiting for transfers between devices, rows_first(): out, at, outs = (lax.all_gather(both, axis, axis=0, tiled=True), 0, [])  138 us
    all_to_all x2, waiting for transfers between devices, summed_on_arrival(): lax.all_to_all(pieces, axis, split_axis=0, concat_axis=0, tiled=True)  40 us
    all_to_all x2, blocking collectives, sent_to_all(): return lax.all_to_all(copies, axis, split_axis=0, concat_axis=0, tiled=True)  31.3 us
    all_to_all x2, waiting for transfers between devices, sent_to_all(): return lax.all_to_all(copies, axis, split_axis=0, concat_axis=0, tiled=True)  20.3 us
    all_to_all x2, starting transfers between devices, sent_to_all(): return lax.all_to_all(copies, axis, split_axis=0, concat_axis=0, tiled=True)  7.77 us
    all_to_all x2, starting transfers between devices, summed_on_arrival(): lax.all_to_all(pieces, axis, split_axis=0, concat_axis=0, tiled=True)  7.13 us
    reduce_sum x2, other arithmetic, on_device(): jnp.sum(conv_out, axis=1)  6.63 us
  transfers between devices with their start and end apart: 8, of which 7 were waited for; matrix products, arithmetic and copies ran while one was open for 4% of the time, Pallas kernels for 0%

commit v1 on v0

--- a/solution.py
+++ b/solution.py
@@ -6,10 +6,15 @@
 epsilon = 1e-06
 
 
+def gather_over(value, axis, dim):
+    sent = jnp.stack([value] * lax.axis_size(axis))
+    return jnp.concatenate(lax.all_to_all(sent, axis, 0, 0), axis=dim)
+
+
 def rows_first(arrays, axis, dims):
     turned = [jnp.moveaxis(a, dim, 0) for a, dim in zip(arrays, dims)]
     both = jnp.concatenate([t.reshape(len(t), -1) for t in turned], axis=1)
-    out, at, outs = (lax.all_gather(both, axis, axis=0, tiled=True), 0, [])
+    out, at, outs = (gather_over(both, axis, 0), 0, [])
     for t, dim in zip(turned, dims):
         slab = out[:, at : at + t[0].size].reshape(-1, *t.shape[1:])
         outs.append(jnp.moveaxis(slab, 0, dim))

time: 316 us -> 462 us (1.46)
  the two profiles are of different devices: /device:TPU:36 before, /device:TPU:6 now
where the time goes in v1:
time: 462 us; the launch traced here: 461 us
  waiting for transfers between devices  341 us (74%)
  starting transfers between devices  41.1 us (9%)
  local copies, waits for them, and re-layouts  31.8 us (7%)
  blocking collectives  27.3 us (6%)
  other arithmetic  10.4 us (2%)
  matrix products  8.18 us (2%)
    all_to_all x1, waiting for transfers between devices, gather_over(): return jnp.concatenate(lax.all_to_all(sent, axis, 0, 0), axis=dim)  269 us
    all_to_all x2, waiting for transfers between devices, summed_on_arrival(): lax.all_to_all(pieces, axis, split_axis=0, concat_axis=0, tiled=True)  39.5 us
    all_to_all x2, blocking collectives, sent_to_all(): return lax.all_to_all(copies, axis, split_axis=0, concat_axis=0, tiled=True)  27.3 us
    all_to_all x2, waiting for transfers between devices, sent_to_all(): return lax.all_to_all(copies, axis, split_axis=0, concat_axis=0, tiled=True)  23.8 us
    all_to_all x1, starting transfers between devices, gather_over(): return jnp.concatenate(lax.all_to_all(sent, axis, 0, 0), axis=dim)  19.9 us
    slice x3, local copies, waits for them, and re-layouts, rows_first(): slab = out[:, at:at + t[0].size].reshape(-1, *t.shape[1:])  13.3 us
  transfers between devices with their start and end apart: 8, of which 8 were waited for; matrix products, arithmetic and copies ran while one was open for 1% of the time, Pallas kernels for 0%

profile of v1, /device:TPU:6, one launch (start us, length us, event | category | flops | bytes accessed | tf_op | source)
XLA Modules:
  0.0 460.6 jit_solution(16711752827725216015)
XLA Ops:
  2.2 3.4 stack.2
  5.6 19.9 %all-to-all-start = ((bf16[128,16,1536]{2,1,0:T(8,128)(2,1)}), bf16[128,16,1536]{2,1,0:T(8,128)(2,1)}, u32[]{:S(2)}, u32[]{:S(2)}) async-start(bf16[128,16,1536]{2,1,0:T(8,128)(2,1)} %stack.2), calls=%async_computation | async-start | bytes 12582912 | tf_op jit(solution)/shard_map/all_to_all | solution.py:11
  28.2 2.7 collective-permute-done.1
  31.1 269.4 %all-to-all-done = bf16[128,16,1536]{2,1,0:T(8,128)(2,1)} async-done(((bf16[128,16,1536]{2,1,0:T(8,128)(2,1)}), bf16[128,16,1536]{2,1,0:T(8,128)(2,1)}, u32[]{:S(2)}, u32[]{:S(2)}) %all-to-all-start) | async-done | bytes 6291488 | tf_op jit(solution)/shard_map/all_to_all | solution.py:11
  300.5 5.4 %fusion.160 = (bf16[2048,512]{1,0:T(8,128)(2,1)}, bf16[2048,512]{1,0:T(8,128)(2,1)S(1)}, bf16[2048,512]{1,0:T(8,128)(2,1)}) fusion(bf16[2048,1536]{1,0:T(8,128)(2,1)} %bitcast.6), kind=kLoop, calls=%fused_computation.286 | loop fusion | bytes 12582912 | tf_op jit(solution)/shard_map/slice | solution.py:19
  306.0 3.9 copy.87
  309.9 4.0 copy.89
  313.9 2.5 fusion.21
  319.4 3.0 collective-permute-done
  322.5 3.3 fusion.157
  326.5 4.5 all-to-all-start.1
  331.0 2.5 copy.102
  333.4 2.8 all-to-all-done.1
  339.5 3.6 all-to-all-start.2
  343.0 21.8 %all-to-all-done.2 = bf16[4,384,512]{2,1,0:T(8,128)(2,1)S(1)} async-done(((bf16[4,384,512]{2,1,0:T(8,128)(2,1)}), bf16[4,384,512]{2,1,0:T(8,128)(2,1)S(1)}, u32[]{:S(2)}, u32[]{:S(2)}) %all-to-all-start.2) | async-done | bytes 1572896 | tf_op jit(solution)/shard_map/all_to_all | solution.py:57
  367.7 3.6 all-to-all-start.3
  371.2 20.9 %all-to-all-done.3 = bf16[4,384,512]{2,1,0:T(8,128)(2,1)S(1)} async-done(((bf16[4,384,512]{2,1,0:T(8,128)(2,1)}), bf16[4,384,512]{2,1,0:T(8,128)(2,1)S(1)}, u32[]{:S(2)}, u32[]{:S(2)}) %all-to-all-start.3) | async-done | bytes 1572896 | tf_op jit(solution)/shard_map/all_to_all | solution.py:33
  396.9 2.1 collective-permute-start.2
  399.1 2.9 collective-permute-done.2
  402.0 3.3 fusion.156
  405.4 7.7 %all_to_all.37 = f32[4,1,768]{2,1,0:T(1,128)S(1)} all-to-all(f32[4,1,768]{2,1,0:T(1,128)S(1)} %broadcast_in_dim.425), channel_id=1, replica_groups=mesh['sp'=128,'tp'=4] {'tp'}, dimensions={0} | all-to-all | bytes 24576 | tf_op jit(solution)/shard_map/all_to_all | solution.py:33
  416.3 3.6 all-to-all-start.5
  420.1 17.8 %all-to-all-done.5 = bf16[4,384,512]{2,1,0:T(8,128)(2,1)S(1)} async-done(((bf16[4,384,512]{2,1,0:T(8,128)(2,1)}), bf16[4,384,512]{2,1,0:T(8,128)(2,1)S(1)}, u32[]{:S(2)}, u32[]{:S(2)}) %all-to-all-start.5) | async-done | bytes 1572896 | tf_op jit(solution)/shard_map/all_to_all | solution.py:57
  438.5 19.6 %all_to_all.38 = bf16[4,384,512]{2,1,0:T(8,128)(2,1)S(1)} all-to-all(bf16[4,384,512]{2,1,0:T(8,128)(2,1)S(1)} %broadcast_in_dim.426), channel_id=1, replica_groups=mesh['sp'=128,'tp'=4] {'tp'}, dimensions={0} | all-to-all | bytes 3145728 | tf_op jit(solution)/shard_map/all_to_all | solution.py:33
  (73 shorter events, 25.9 us)
Async XLA Ops:
  5.6 19.9 %copy-start.6 = (s32[384]{0:T(512)S(1)}, s32[384]{0:T(512)}, u32[]{:S(2)}) copy-start(s32[384]{0:T(512)} %param.10) | copy-start | bytes 4612
  5.6 22.0 %copy-start = (bf16[384,2048]{1,0:T(8,128)(2,1)S(1)}, bf16[384,2048]{1,0:T(8,128)(2,1)}, u32[]{:S(2)}) copy-start(bf16[384,2048]{1,0:T(8,128)(2,1)} %param.9) | copy-start | bytes 4718596
  5.6 22.5 %copy-start.5 = (f32[2,31,256]{2,0,1:T(2,128)S(1)}, f32[2,31,256]{2,0,1:T(2,128)}, u32[]{:S(2)}) copy-start(f32[2,31,256]{2,0,1:T(2,128)} %param.15) | copy-start | bytes 190468
  5.6 22.5 %copy-start.7 = (f32[2,2048]{1,0:T(2,128)S(1)}, f32[2,2048]{1,0:T(2,128)}, u32[]{:S(2)}) copy-start(f32[2,2048]{1,0:T(2,128)} %param.11) | copy-start | bytes 49156
  5.6 22.6 %copy-start.8 = (f32[2,256]{1,0:T(2,128)S(1)}, f32[2,256]{1,0:T(2,128)}, u32[]{:S(2)}) copy-start(f32[2,256]{1,0:T(2,128)} %param.16) | copy-start | bytes 6148
  5.6 294.9 %all-to-all-start = ((bf16[128,16,1536]{2,1,0:T(8,128)(2,1)}), bf16[128,16,1536]{2,1,0:T(8,128)(2,1)}, u32[]{:S(2)}, u32[]{:S(2)}) async-start(bf16[128,16,1536]{2,1,0:T(8,128)(2,1)} %stack.2), calls=%async_computation | async-start | bytes 12582912 | tf_op jit(solution)/shard_map/all_to_all | solution.py:11
  25.6 5.3 %collective-permute-start.1 = (s32[30]{0:T(128)S(1)}, s32[30]{0:T(128)S(1)}, u32[]{:S(2)}, u32[]{:S(2)}) collective-permute-start(s32[30]{0:T(128)S(1)} %slice.568), channel_id=1, source_target_pairs={{0,4},{4,8},{8,12},{12,16},{16,20},{20,24},{24,28},{28,32},{32,36}... | collective-permute-start | bytes 368 | tf_op jit(solution)/shard_map/ppermute | solution.py:28
  313.9 2.5 copy-start.1
  313.9 2.9 copy-start.3
  317.4 5.1 %collective-permute-start = (bf16[30,256]{1,0:T(8,128)(2,1)S(1)}, bf16[30,256]{1,0:T(8,128)(2,1)S(1)}, u32[]{:S(2)}, u32[]{:S(2)}) collective-permute-start(bf16[30,256]{1,0:T(8,128)(2,1)S(1)} %slice.739), channel_id=1, source_target_pairs={{0,4},{4,8},{8,12},{12,16},{16,20},{20,24},{24,28},{28,32},{32,36}... | collective-permute-start | bytes 46088 | tf_op jit(solution)/shard_map/ppermute | solution.py:28
  322.5 8.4 %copy-start.9 = (f32[2,256]{1,0:T(2,128)S(1)}, f32[2,256]{1,0:T(2,128)}, u32[]{:S(2)}) copy-start(f32[2,256]{1,0:T(2,128)} %param.17) | copy-start | bytes 6148
  326.5 9.8 %all-to-all-start.1 = ((f32[4,1,768]{2,1,0:T(1,128)}), f32[4,1,768]{2,1,0:T(1,128)S(1)}, u32[]{:S(2)}, u32[]{:S(2)}) async-start(f32[4,1,768]{2,1,0:T(1,128)} %broadcast_in_dim.423), calls=%async_computation.1 | async-start | bytes 24576 | tf_op jit(solution)/shard_map/all_to_all | solution.py:33
  339.5 25.4 %all-to-all-start.2 = ((bf16[4,384,512]{2,1,0:T(8,128)(2,1)}), bf16[4,384,512]{2,1,0:T(8,128)(2,1)S(1)}, u32[]{:S(2)}, u32[]{:S(2)}) async-start(bf16[4,384,512]{2,1,0:T(8,128)(2,1)} %bitcast.132), calls=%async_computation.2 | async-start | bytes 3145728 | tf_op jit(solution)/shard_map/all_to_all | solution.py:57
  367.7 24.5 %all-to-all-start.3 = ((bf16[4,384,512]{2,1,0:T(8,128)(2,1)}), bf16[4,384,512]{2,1,0:T(8,128)(2,1)S(1)}, u32[]{:S(2)}, u32[]{:S(2)}) async-start(bf16[4,384,512]{2,1,0:T(8,128)(2,1)} %broadcast_in_dim.424), calls=%async_computation.3 | async-start | bytes 3145728 | tf_op jit(solution)/shard_map/all_to_all | solution.py:33
  393.1 1.6 copy-start.2
  394.6 1.6 copy-start.4
  396.9 5.1 %collective-permute-start.2 = (bf16[30,256]{1,0:T(8,128)(2,1)S(1)}, bf16[30,256]{1,0:T(8,128)(2,1)S(1)}, u32[]{:S(2)}, u32[]{:S(2)}) collective-permute-start(bf16[30,256]{1,0:T(8,128)(2,1)S(1)} %slice.775), channel_id=1, source_target_pairs={{0,4},{4,8},{8,12},{12,16},{16,20},{20,24},{24,28},{28,32},{32,36}... | collective-permute-start | bytes 46088 | tf_op jit(solution)/shard_map/ppermute | solution.py:28
  416.3 21.6 %all-to-all-start.5 = ((bf16[4,384,512]{2,1,0:T(8,128)(2,1)}), bf16[4,384,512]{2,1,0:T(8,128)(2,1)S(1)}, u32[]{:S(2)}, u32[]{:S(2)}) async-start(bf16[4,384,512]{2,1,0:T(8,128)(2,1)} %bitcast.134), calls=%async_computation.5 | async-start | bytes 3145728 | tf_op jit(solution)/shard_map/all_to_all | solution.py:57
